TPU v7x, 512 devices: a whole 4x4x16 slice. The times are simulated.
512 devices in a mesh: sp: 16 (over z), fs: 4 (over y), tp: 8 (over x, core).
Axes of the slice: x: 4, y: 4, z: 16, core: 2. Of those that a mesh axis runs over, the one named last changes fastest.
Arguments:
- tokens: bfloat16 [4, 16384, 2048], P('fs', ('sp', 'tp')), may hold values from -6 to 6
- input_norm_gain: float32 [2048], replicated, may hold values from 0.1 to 1.9
- earlier_gate: bfloat16 [2048, 1024], P(('sp', 'fs'), 'tp'), may hold values from -0.125 to 0.125
- later_gate: bfloat16 [2048, 1024], P(('sp', 'fs'), 'tp'), may hold values from -0.125 to 0.125
- convolution_input: bfloat16 [2048, 1024], P(('sp', 'fs'), 'tp'), may hold values from -0.125 to 0.125
- convolution_taps: float32 [3, 1024], P(None, 'tp'), may hold values from -3 to 3
- receptance: bfloat16 [2048, 1024], P(('sp', 'fs'), 'tp'), may hold values from -0.125 to 0.125
- key_matrix: bfloat16 [2048, 1024], P(('sp', 'fs'), 'tp'), may hold values from -0.125 to 0.125
- value_matrix: bfloat16 [2048, 1024], P(('sp', 'fs'), 'tp'), may hold values from -0.125 to 0.125
- decay_matrix: bfloat16 [2048, 1024], P(('sp', 'fs'), 'tp'), may hold values from -0.125 to 0.125
- rate_matrix: bfloat16 [2048, 1024], P(('sp', 'fs'), 'tp'), may hold values from -0.125 to 0.125
- decay_floor: float32 [1024], P('tp'), may hold values from -16 to -3.4
- rate_offset: float32 [1024], P('tp'), may hold values from -7.5 to 1
- decay_spike: float32 [4, 16384, 1024], P('fs', 'sp', 'tp'), may hold values from -1.3 to 0
- initial_state: float32 [4, 16, 64, 64], P('fs', 'tp'), may hold values from -768 to 768
- head_norm_gain: float32 [1024], P('tp'), may hold values from 0.1 to 1.9
- convolution_output: bfloat16 [1024, 2048], P('tp', ('sp', 'fs')), may hold values from -0.125 to 0.125
- state_heads_output: bfloat16 [1024, 2048], P('tp', ('sp', 'fs')), may hold values from -0.125 to 0.125
Outputs:
- mixed: bfloat16 [4, 16384, 2048], P('fs', ('sp', 'tp'))
All inputs are finite; a program needn't handle non-finite values.
Results may differ from a plain program's by a relative error of at most 0.02.
Values may be sent and summed in bfloat16 or wider, within the bound.
No kernel may reach another device: no remote copies, remote signals or barrier semaphores. Data moves between devices by JAX's collectives and lax.ppermute only.
A program may use at most 64 MiB of HBM per device.

v0:
```python
import jax
import jax.numpy as jnp
from jax import lax
from jax.sharding import PartitionSpec as P

HEAD_WIDTH = 64
BLOCK = 64
norm_eps = 1e-06
key_eps = 1e-06


def passed_along(block, axis, distance):
    devices = range(lax.axis_size(axis))
    route = [(i - distance, i) for i in devices if i - distance in devices]
    return lax.ppermute(block, axis, route)


def side_by_side(arrays, axis, dim, along):
    widths = [a.shape[along] for a in arrays]
    both = jnp.concatenate(arrays, axis=along)
    out = lax.all_gather(both, axis, axis=dim, tiled=True)
    return tuple(jnp.split(out, [sum(widths[:k]) for k in range(1, len(widths))], axis=along))


def from_everyone(x, axis):
    devices = lax.axis_size(axis)
    return lax.all_to_all(jnp.broadcast_to(x[None], (devices, *x.shape)), axis, 0, 0, tiled=True)


def collected_together(x, axis):
    leaves = jax.tree.leaves(x)
    order = sorted(range(len(leaves)), key=lambda k: -leaves[k].size)
    width = (1, *leaves[order[0]].shape)[-1]
    lines = [
        jnp.pad(leaves[k].reshape(-1), (0, -leaves[k].size % width)).reshape(-1, width)
        for k in order
    ]
    both, at, found = (from_everyone(jnp.concatenate(lines), axis), 0, {})
    for k, line in zip(order, lines):
        piece = both[:, at : at + len(line)].reshape(len(both), -1)
        found[k] = piece[:, : leaves[k].size].reshape(-1, *leaves[k].shape)
        at += len(line)
    numbers = iter(range(len(leaves)))
    return jax.tree.map(lambda _: found[next(numbers)], x)


def combined_pairwise(pieces, combine):
    while len(jax.tree.leaves(pieces)[0]) > 1:
        pieces = jax.vmap(combine)(
            *(jax.tree.map(lambda part: part[side::2], pieces) for side in (0, 1))
        )
    return jax.tree.map(lambda part: part[0], pieces)


def entering(x, axis, combine, identity):
    devices, position = (lax.axis_size(axis), lax.axis_index(axis))
    passed = jnp.arange(devices) < position

    def kept(part, zero, own):
        part = jnp.where(
            passed.reshape(-1, *(1 for _ in own.shape)),
            part.astype(own.dtype),
            jnp.asarray(zero, own.dtype),
        )
        return part

    pieces = collected_together(
        jax.tree.map(lambda part, kind: part.astype(kind), x, (jnp.bfloat16, jnp.bfloat16)), axis
    )
    return combined_pairwise(jax.tree.map(kept, pieces, identity, x), combine)


def gather_turned(arrays, axis, dims):
    turned = [jnp.moveaxis(a, dim, 0) for a, dim in zip(arrays, dims)]
    both = jnp.concatenate([t.reshape(len(t), -1) for t in turned], axis=1)
    out, at, outs = (lax.all_gather(both, axis, axis=0, tiled=True), 0, [])
    for t, dim in zip(turned, dims):
        piece = out[:, at : at + t[0].size].reshape(-1, *t.shape[1:])
        outs.append(jnp.moveaxis(piece, 0, dim))
        at += t[0].size
    return tuple(outs)


def rms_rows(activations, gain_vector):
    values = activations.astype(jnp.float32)
    inv_scale = lax.rsqrt(jnp.mean(values * values, axis=-1, keepdims=True) + norm_eps)
    return (values * inv_scale * gain_vector).astype(jnp.bfloat16)


def project(activations, weight):
    return jnp.dot(activations, weight, preferred_element_type=jnp.float32).astype(jnp.bfloat16)


def conv_branch(pre_values, post_values, conv_values, convolution_taps):
    product = pre_values.astype(jnp.float32) * conv_values.astype(jnp.float32)
    reach_rows = convolution_taps.shape[0] - 1
    sequence_rows = product.shape[0]
    edge_rows = passed_along(product[sequence_rows - reach_rows :], "sp", 1)
    padded = jnp.concatenate([edge_rows, product], axis=0)
    filtered = convolution_taps[0] * padded[0:sequence_rows]
    for offset in range(1, convolution_taps.shape[0]):
        filtered = filtered + convolution_taps[offset] * padded[offset : offset + sequence_rows]
    return (post_values.astype(jnp.float32) * filtered).astype(jnp.bfloat16)


def pairs(left_side, right_side, allowed):
    return jnp.where(allowed, jnp.einsum("thj,shj->hts", left_side, right_side), 0.0)


def block_pass(carried, inputs):
    queries, key_rows, value_rows, unit_keys, beta_rows, logarithm_decay = inputs
    span_rows = logarithm_decay.shape[0]
    cumulative = jnp.cumsum(logarithm_decay, axis=0)
    previous = cumulative - logarithm_decay
    middle = cumulative[span_rows // 2]
    later_index = lax.broadcasted_iota(jnp.int32, (span_rows, span_rows), 0)
    earlier_index = lax.broadcasted_iota(jnp.int32, (span_rows, span_rows), 1)
    strict = (later_index > earlier_index)[None]
    inclusive = (later_index >= earlier_index)[None]
    ask_keys = unit_keys * jnp.exp(previous - middle)
    ask_reads = queries * jnp.exp(cumulative - middle)
    give_keys = key_rows * jnp.exp(middle - cumulative)
    give_betas = beta_rows * jnp.exp(middle - cumulative)
    key_ask = pairs(ask_keys, give_keys, strict)
    beta_ask = pairs(ask_keys, give_betas, strict)
    key_read = pairs(ask_reads, give_keys, inclusive)
    beta_read = pairs(ask_reads, give_betas, inclusive)
    extended = jnp.concatenate([value_rows, jnp.zeros_like(value_rows)], axis=2)
    from_start = jnp.einsum("thj,hrj->htr", unit_keys * jnp.exp(previous), carried)
    right_side = from_start + jnp.einsum("hts,shr->htr", key_ask, extended)
    system = beta_ask + jnp.eye(span_rows, dtype=jnp.float32)[None]
    removed = jax.scipy.linalg.solve_triangular(system, right_side, lower=True, unit_diagonal=True)
    outputs = (
        jnp.einsum("thj,hrj->thr", queries * jnp.exp(cumulative), carried)
        + jnp.einsum("hts,shr->thr", key_read, extended)
        - jnp.einsum("hts,hsr->thr", beta_read, removed)
    )
    closing = cumulative[span_rows - 1]
    tail_decay = jnp.exp(closing - cumulative)
    carried = (
        carried * jnp.exp(closing)[:, None, :]
        + jnp.einsum("shr,shj->hrj", extended, key_rows * tail_decay)
        - jnp.einsum("hsr,shj->hrj", removed, beta_rows * tail_decay)
    )
    return (carried, outputs)


def compose(earlier, later):
    return (
        jnp.einsum("hij,hjk->hik", earlier[0], later[0]),
        jnp.einsum("hij,hjk->hik", earlier[1], later[0]) + later[1],
    )


def on_device(
    tokens,
    input_norm_gain,
    earlier_gate,
    later_gate,
    convolution_input,
    convolution_taps,
    receptance,
    key_matrix,
    value_matrix,
    decay_matrix,
    rate_matrix,
    decay_floor,
    rate_offset,
    decay_spike,
    initial_state,
    head_norm_gain,
    convolution_output,
    state_heads_output,
):
    normed = rms_rows(tokens[0], input_norm_gain)
    channels = earlier_gate.shape[1]
    gathered = side_by_side(
        (
            earlier_gate,
            later_gate,
            convolution_input,
            receptance,
            key_matrix,
            value_matrix,
            decay_matrix,
            rate_matrix,
        ),
        ("sp", "fs"),
        0,
        1,
    )
    piece = lax.all_gather(normed, "tp", axis=0, tiled=True)
    projected = jnp.concatenate([project(piece, weight) for weight in gathered], axis=1)
    pieces = jnp.split(projected, 8, axis=1)
    conv_mixed = conv_branch(pieces[0], pieces[1], pieces[2], convolution_taps)
    queries_raw, keys_raw, values_raw, decay_pre, rate_pre = pieces[3:]
    sequence_rows = queries_raw.shape[0]
    present_heads = channels // HEAD_WIDTH

    def by_heads(array):
        return array.astype(jnp.float32).reshape(sequence_rows, present_heads, HEAD_WIDTH)

    queries = by_heads(queries_raw)
    key_rows = by_heads(keys_raw)
    value_rows = by_heads(values_raw)
    logarithm_decay = -jnp.exp(
        decay_floor.reshape(present_heads, HEAD_WIDTH) + jnp.tanh(by_heads(decay_pre))
    )
    logarithm_decay = logarithm_decay + decay_spike[0].reshape(
        sequence_rows, present_heads, HEAD_WIDTH
    )
    learn_rate = jax.nn.sigmoid(rate_offset.reshape(present_heads, HEAD_WIDTH) + by_heads(rate_pre))
    unit_keys = key_rows * lax.rsqrt(jnp.sum(key_rows * key_rows, axis=-1, keepdims=True) + key_eps)
    beta_rows = learn_rate * unit_keys
    blocks = sequence_rows // BLOCK

    def in_blocks(array):
        return array.reshape(blocks, BLOCK, present_heads, HEAD_WIDTH)

    identity = jnp.broadcast_to(
        jnp.eye(HEAD_WIDTH, dtype=jnp.float32), (present_heads, HEAD_WIDTH, HEAD_WIDTH)
    )
    initial_rows = jnp.concatenate(
        [jnp.zeros((present_heads, HEAD_WIDTH, HEAD_WIDTH), jnp.float32), identity], axis=1
    )
    ending, outputs = lax.scan(
        block_pass,
        initial_rows,
        tuple(
            (
                in_blocks(array)
                for array in (queries, key_rows, value_rows, unit_keys, beta_rows, logarithm_decay)
            )
        ),
    )
    outputs = outputs.reshape(sequence_rows, present_heads, 2 * HEAD_WIDTH)
    carry_source = ending[:, :HEAD_WIDTH, :]
    carry_map = ending[:, HEAD_WIDTH:, :]
    first_state = initial_state[0]
    prefix_map, prefix_source = entering(
        (carry_map, carry_source), "sp", compose, (identity, jnp.zeros_like(carry_source))
    )
    opening_state = jnp.einsum("hvj,hjk->hvk", first_state, prefix_map) + prefix_source
    reads = outputs[..., :HEAD_WIDTH] + jnp.einsum(
        "thj,hvj->thv", outputs[..., HEAD_WIDTH:], opening_state
    )
    centered = reads - jnp.mean(reads, axis=-1, keepdims=True)
    variance = jnp.mean(centered * centered, axis=-1, keepdims=True)
    state_mixed = (
        centered
        * lax.rsqrt(variance + HEAD_WIDTH * 1e-05)
        * head_norm_gain.reshape(present_heads, HEAD_WIDTH)
    )
    state_mixed = state_mixed.reshape(sequence_rows, channels).astype(jnp.bfloat16)
    conv_whole, state_whole = gather_turned(
        (convolution_output, state_heads_output), ("sp", "fs"), (1, 1)
    )
    mixed = lax.psum_scatter(
        (
            jnp.dot(conv_mixed, conv_whole, preferred_element_type=jnp.float32)
            + jnp.dot(state_mixed, state_whole, preferred_element_type=jnp.float32)
        ).astype(jnp.bfloat16),
        "tp",
        scatter_dimension=0,
        tiled=True,
    )
    return mixed[None]


def solution(mesh):
    placed = (
        P("fs", ("sp", "tp"), None),
        P(),
        P(("sp", "fs"), "tp"),
        P(("sp", "fs"), "tp"),
        P(("sp", "fs"), "tp"),
        P(None, "tp"),
        P(("sp", "fs"), "tp"),
        P(("sp", "fs"), "tp"),
        P(("sp", "fs"), "tp"),
        P(("sp", "fs"), "tp"),
        P(("sp", "fs"), "tp"),
        P("tp"),
        P("tp"),
        P("fs", "sp", "tp"),
        P("fs", "tp", None, None),
        P("tp"),
        P("tp", ("sp", "fs")),
        P("tp", ("sp", "fs")),
    )
    return jax.shard_map(
        on_device,
        mesh=mesh,
        in_specs=placed,
        out_specs=P("fs", ("sp", "tp"), None),
        check_vma=False,
    )
```

profile of v0, /device:TPU:8, one launch (start us, length us, event | category | flops | bytes accessed | tf_op | source)
XLA Modules:
  0.0 573.6 jit_solution(10139626129675810700)
XLA Ops:
  6.5 1.3 fusion.63
  7.8 2.0 fusion.65
  16.2 1.3 pad_maximum_fusion.2
  18.3 2.6 reshape_squeeze.3
  21.9 32.2 %all-gather.4.cloned.1.call-done = bf16[1024,2048]{1,0:T(8,128)(2,1)} async-done(((bf16[128,2048]{1,0:T(8,128)(2,1)}), bf16[1024,2048]{1,0:T(8,128)(2,1)}) %all-gather.4.cloned.1.call-update) | async-done | bytes 4194320 | tf_op jit(solution)/shard_map/all_gather | solution.py:192
  54.1 147.6 %all-gather.6.cloned.1.call-done = bf16[2048,1024]{1,0:T(8,128)(2,1)} async-done(((bf16[32,1024]{1,0:T(8,128)(2,1)}), bf16[2048,1024]{1,0:T(8,128)(2,1)}) %all-gather.6.cloned.1.call-update) | async-done | bytes 4194320 | tf_op jit(solution)/shard_map/all_gather | solution.py:21
  201.7 3.8 bitcast_reduce_fusion
  207.5 4.3 fusion.51
  211.9 1.6 reshape.141
  213.5 4.4 fusion.55
  217.9 2.7 tanh.8
  220.5 4.3 fusion.50
  224.9 2.6 reshape.142
  227.5 4.3 fusion.53
  231.8 2.0 reshape.139
  233.8 2.7 negate_add_fusion
  236.5 4.0 divide_multiply_fusion
  240.5 237.3 %while.12 = (s32[]{:T(128)}, f32[2,128,64]{1,2,0:T(8,128)S(1)}, f32[16,64,2,128]{3,1,0,2:T(8,128)S(1)}, f32[16,64,2,64]{3,2,1,0:T(2,128)}, bf16[16,64,2,64]{3,2,...) while((s32[]{:T(128)}, f32[2,128,64]{1,2,0:T(8,128)S(1)}, ...), condition=%wide.region_4.5_spmd, body=%wide.region_2.4_spmd.sunk | while | flops 32329792 | bytes 2025073 | solution.py:226
  241.4 1.2 bitcast_multiply_fusion.9
  244.1 9.8 %custom-call.8 = f32[2,1,64,64]{2,3,1,0:T(8,128)S(1)} custom-call(f32[2,1,64,64]{3,2,1,0:T(8,128)S(1)} %fusion.192), custom_call_target="InvertDiagBlocksLowerTriangular" | custom-call | tf_op jit(solution)/shard_map/while/body/eval_jaxpr/jit(_solve_triangular)/vmap()/triangular_solve | solution.py:132
  256.3 1.2 bitcast_multiply_fusion.9
  259.0 9.8 %custom-call.8 = f32[2,1,64,64]{2,3,1,0:T(8,128)S(1)} custom-call(f32[2,1,64,64]{3,2,1,0:T(8,128)S(1)} %fusion.192), custom_call_target="InvertDiagBlocksLowerTriangular" | custom-call | tf_op jit(solution)/shard_map/while/body/eval_jaxpr/jit(_solve_triangular)/vmap()/triangular_solve | solution.py:132
  271.1 1.2 bitcast_multiply_fusion.9
  273.8 9.8 %custom-call.8 = f32[2,1,64,64]{2,3,1,0:T(8,128)S(1)} custom-call(f32[2,1,64,64]{3,2,1,0:T(8,128)S(1)} %fusion.192), custom_call_target="InvertDiagBlocksLowerTriangular" | custom-call | tf_op jit(solution)/shard_map/while/body/eval_jaxpr/jit(_solve_triangular)/vmap()/triangular_solve | solution.py:132
  285.9 1.2 bitcast_multiply_fusion.9
  288.6 9.9 %custom-call.8 = f32[2,1,64,64]{2,3,1,0:T(8,128)S(1)} custom-call(f32[2,1,64,64]{3,2,1,0:T(8,128)S(1)} %fusion.192), custom_call_target="InvertDiagBlocksLowerTriangular" | custom-call | tf_op jit(solution)/shard_map/while/body/eval_jaxpr/jit(_solve_triangular)/vmap()/triangular_solve | solution.py:132
  303.5 9.9 %custom-call.8 = f32[2,1,64,64]{2,3,1,0:T(8,128)S(1)} custom-call(f32[2,1,64,64]{3,2,1,0:T(8,128)S(1)} %fusion.192), custom_call_target="InvertDiagBlocksLowerTriangular" | custom-call | tf_op jit(solution)/shard_map/while/body/eval_jaxpr/jit(_solve_triangular)/vmap()/triangular_solve | solution.py:132
  318.3 9.8 %custom-call.8 = f32[2,1,64,64]{2,3,1,0:T(8,128)S(1)} custom-call(f32[2,1,64,64]{3,2,1,0:T(8,128)S(1)} %fusion.192), custom_call_target="InvertDiagBlocksLowerTriangular" | custom-call | tf_op jit(solution)/shard_map/while/body/eval_jaxpr/jit(_solve_triangular)/vmap()/triangular_solve | solution.py:132
  333.1 9.8 %custom-call.8 = f32[2,1,64,64]{2,3,1,0:T(8,128)S(1)} custom-call(f32[2,1,64,64]{3,2,1,0:T(8,128)S(1)} %fusion.192), custom_call_target="InvertDiagBlocksLowerTriangular" | custom-call | tf_op jit(solution)/shard_map/while/body/eval_jaxpr/jit(_solve_triangular)/vmap()/triangular_solve | solution.py:132
  347.9 9.8 %custom-call.8 = f32[2,1,64,64]{2,3,1,0:T(8,128)S(1)} custom-call(f32[2,1,64,64]{3,2,1,0:T(8,128)S(1)} %fusion.192), custom_call_target="InvertDiagBlocksLowerTriangular" | custom-call | tf_op jit(solution)/shard_map/while/body/eval_jaxpr/jit(_solve_triangular)/vmap()/triangular_solve | solution.py:132
  362.8 9.8 %custom-call.8 = f32[2,1,64,64]{2,3,1,0:T(8,128)S(1)} custom-call(f32[2,1,64,64]{3,2,1,0:T(8,128)S(1)} %fusion.192), custom_call_target="InvertDiagBlocksLowerTriangular" | custom-call | tf_op jit(solution)/shard_map/while/body/eval_jaxpr/jit(_solve_triangular)/vmap()/triangular_solve | solution.py:132
  374.9 1.2 bitcast_multiply_fusion.9
  377.6 9.8 %custom-call.8 = f32[2,1,64,64]{2,3,1,0:T(8,128)S(1)} custom-call(f32[2,1,64,64]{3,2,1,0:T(8,128)S(1)} %fusion.192), custom_call_target="InvertDiagBlocksLowerTriangular" | custom-call | tf_op jit(solution)/shard_map/while/body/eval_jaxpr/jit(_solve_triangular)/vmap()/triangular_solve | solution.py:132
  392.4 9.8 %custom-call.8 = f32[2,1,64,64]{2,3,1,0:T(8,128)S(1)} custom-call(f32[2,1,64,64]{3,2,1,0:T(8,128)S(1)} %fusion.192), custom_call_target="InvertDiagBlocksLowerTriangular" | custom-call | tf_op jit(solution)/shard_map/while/body/eval_jaxpr/jit(_solve_triangular)/vmap()/triangular_solve | solution.py:132
  407.3 9.8 %custom-call.8 = f32[2,1,64,64]{2,3,1,0:T(8,128)S(1)} custom-call(f32[2,1,64,64]{3,2,1,0:T(8,128)S(1)} %fusion.192), custom_call_target="InvertDiagBlocksLowerTriangular" | custom-call | tf_op jit(solution)/shard_map/while/body/eval_jaxpr/jit(_solve_triangular)/vmap()/triangular_solve | solution.py:132
  419.4 1.2 bitcast_multiply_fusion.9
  422.1 9.8 %custom-call.8 = f32[2,1,64,64]{2,3,1,0:T(8,128)S(1)} custom-call(f32[2,1,64,64]{3,2,1,0:T(8,128)S(1)} %fusion.192), custom_call_target="InvertDiagBlocksLowerTriangular" | custom-call | tf_op jit(solution)/shard_map/while/body/eval_jaxpr/jit(_solve_triangular)/vmap()/triangular_solve | solution.py:132
  436.9 9.8 %custom-call.8 = f32[2,1,64,64]{2,3,1,0:T(8,128)S(1)} custom-call(f32[2,1,64,64]{3,2,1,0:T(8,128)S(1)} %fusion.192), custom_call_target="InvertDiagBlocksLowerTriangular" | custom-call | tf_op jit(solution)/shard_map/while/body/eval_jaxpr/jit(_solve_triangular)/vmap()/triangular_solve | solution.py:132
  451.7 9.8 %custom-call.8 = f32[2,1,64,64]{2,3,1,0:T(8,128)S(1)} custom-call(f32[2,1,64,64]{3,2,1,0:T(8,128)S(1)} %fusion.192), custom_call_target="InvertDiagBlocksLowerTriangular" | custom-call | tf_op jit(solution)/shard_map/while/body/eval_jaxpr/jit(_solve_triangular)/vmap()/triangular_solve | solution.py:132
  463.9 1.2 bitcast_multiply_fusion.9
  466.6 9.8 %custom-call.8 = f32[2,1,64,64]{2,3,1,0:T(8,128)S(1)} custom-call(f32[2,1,64,64]{3,2,1,0:T(8,128)S(1)} %fusion.192), custom_call_target="InvertDiagBlocksLowerTriangular" | custom-call | tf_op jit(solution)/shard_map/while/body/eval_jaxpr/jit(_solve_triangular)/vmap()/triangular_solve | solution.py:132
  479.0 7.5 %all-to-all-start = ((bf16[16,256,64]{1,2,0:T(8,128)(2,1)}), bf16[16,256,64]{1,2,0:T(8,128)(2,1)S(1)}, u32[]{:S(2)}, u32[]{:S(2)}) async-start(bf16[16,256,64]{1,2,0:T(8,128)(2,1)} %broadcast_in_dim.79), calls=%async_computation | async-start | bytes 1048576 | tf_op jit(solution)/shard_map/all_to_all | solution.py:27
  486.8 3.7 fusion.58
  490.5 2.3 fusion.57
  492.9 3.8 collective-permute-start
  498.0 10.0 %fusion.79 = f32[1024,2048]{1,0:T(8,128)} fusion(bf16[2048,256]{1,0:T(8,128)(2,1)} %all-gather.8.cloned.1.call-done, f32[2,128]{1,0:T(2,128)S(1)} %collective-permute-done, f32[1024,128]{1,0:T(8,128)S(1)} %fusion.57, bf16[1024,2048]{1,0:T(8,128)(2,1)} %all-gather.4.cloned.1.call-done, bf16[2048,1024]{1,0:T(8,128)(2,1)} %all-gather.6.cloned.1.call-done, ...), kind=kOutput, calls=%fused_computation.125 | convolution fusion | flops 1075183616 | bytes 14158336 | tf_op jit(solution)/shard_map/dot_general | solution.py:260
  511.1 6.8 %add_convert_fusion = bf16[1024,2048]{1,0:T(8,128)(2,1)} fusion(f32[1024,2048]{1,0:T(8,128)} %fusion.79, bf16[1024,128]{0,1:T(8,128)(2,1)S(1)} %bitcast.179, bf16[2048,256]{1,0:T(8,128)(2,1)} %all-gather.8.cloned.1.call-done), kind=kOutput, calls=%fused_computation.74 | convolution fusion | flops 541065216 | bytes 13369344 | tf_op jit(solution)/shard_map/dot_general | solution.py:261
  517.9 49.1 %reduce-scatter.2.cloned.1.call-done = bf16[128,2048]{1,0:T(8,128)(2,1)} async-done(((bf16[1024,2048]{1,0:T(8,128)(2,1)}), bf16[128,2048]{1,0:T(8,128)(2,1)}) %reduce-scatter.2.cloned.1.call-update) | async-done | bytes 524304 | tf_op jit(solution)/shard_map/reduce_scatter | solution.py:258
  (370 shorter events, 85.6 us)
Async XLA Ops:
  6.5 503.9 %copy-start = (f32[1,2,64,64]{3,2,1,0:T(8,128)S(1)}, f32[1,2,64,64]{3,2,1,0:T(8,128)}, u32[]{:S(2)}) copy-start(f32[1,2,64,64]{3,2,1,0:T(8,128)} %param.34) | copy-start | bytes 98308
  6.5 47.6 %all-gather.4.cloned.1.call-start = ((), (), s32[]{:S(2)}) async-start(), calls=%async_computation.2 | async-start | bytes 4718592 | tf_op jit(solution)/shard_map/all_gather | solution.py:192
  9.9 191.9 %all-gather.6.cloned.1.call-start = ((), (), s32[]{:S(2)}) async-start(), calls=%async_computation.3 | async-start | bytes 4259840 | tf_op jit(solution)/shard_map/all_gather | solution.py:21
  15.5 0.6 copy-start.2
  16.2 480.9 %all-gather.8.cloned.1.call-start = ((), (), s32[]{:S(2)}) async-start(), calls=%async_computation.4 | async-start | bytes 1064960 | tf_op jit(solution)/shard_map/all_gather | solution.py:76
  240.5 246.3 %copy-start.3 = (f32[3,128]{1,0:T(4,128)S(1)}, f32[3,128]{1,0:T(4,128)}, u32[]{:S(2)}) copy-start(f32[3,128]{1,0:T(4,128)} %param.25) | copy-start | bytes 4612
  479.0 29.0 %all-to-all-start = ((bf16[16,256,64]{1,2,0:T(8,128)(2,1)}), bf16[16,256,64]{1,2,0:T(8,128)(2,1)S(1)}, u32[]{:S(2)}, u32[]{:S(2)}) async-start(bf16[16,256,64]{1,2,0:T(8,128)(2,1)} %broadcast_in_dim.79), calls=%async_computation | async-start | bytes 1048576 | tf_op jit(solution)/shard_map/all_to_all | solution.py:27
  486.6 80.5 %reduce-scatter.2.cloned.1.call-start = ((), (), s32[]{:S(2)}) async-start(), calls=%async_computation.5 | async-start | bytes 4718592 | tf_op jit(solution)/shard_map/reduce_scatter | solution.py:258
  486.8 3.7 copy-start.1
  490.5 6.2 %copy-start.4 = (f32[128]{0:T(128)S(1)}, f32[128]{0:T(128)}, u32[]{:S(2)}) copy-start(f32[128]{0:T(128)} %param.35) | copy-start | bytes 1540
  492.9 5.1 collective-permute-start
Sparse Core Ops, SparseCore 0:
  10.0 44.0 all-gather.3
  57.0 144.6 all-gather.5
  204.7 136.9 all-gather.7
  518.1 48.9 reduce-scatter.1
where the time goes:
time: 577 us; the launch traced here: 574 us
  waiting for transfers between devices  230 us (40%)
  other arithmetic  205 us (36%)
  matrix products  75.6 us (13%)
  local copies, waits for them, and re-layouts  36.4 us (6%)
  between operations  13.5 us (2%)
  starting transfers between devices  11.7 us (2%)
    another operation x32, other arithmetic, block_pass(): jax.scipy.linalg.solve_triangular(system, right_side, lower=True, unit_di...  157 us
    all_gather x1, waiting for transfers between devices, side_by_side(): out = lax.all_gather(both, axis, axis=dim, tiled=True)  148 us
    reduce_scatter x1, waiting for transfers between devices, on_device(): lax.psum_scatter((jnp.dot(conv_mixed, conv_whole, preferred_element_type=...  49.1 us
    all_gather x1, waiting for transfers between devices, on_device(): piece = lax.all_gather(normed, 'tp', axis=0, tiled=True)  32.2 us
    dot_general x7, matrix products, project(): jnp.dot(activations, weight, preferred_element_type=jnp.float32)  27.1 us
    mul x16, other arithmetic, block_pass(): ask_reads = queries * jnp.exp(cumulative - middle)  19.7 us
    another operation x16, other arithmetic, block_pass(): cumulative = jnp.cumsum(logarithm_decay, axis=0)  14.6 us
    dynamic_slice x32, local copies, waits for them, and re-layouts, on_device(): lax.scan(block_pass, initial_rows, tuple((in_blocks(array) for array in (...  12.7 us
  transfers between devices with their start and end apart: 6, of which 4 were waited for; matrix products, arithmetic and copies ran while one was open for 53% of the time, Pallas kernels for 0%

commit v1 on v0

--- a/solution.py
+++ b/solution.py
@@ -189,7 +189,9 @@
         0,
         1,
     )
-    piece = lax.all_gather(normed, "tp", axis=0, tiled=True)
+    piece = jnp.concatenate(
+        lax.all_to_all(jnp.stack([normed] * lax.axis_size("tp")), "tp", 0, 0), axis=0
+    )
     projected = jnp.concatenate([project(piece, weight) for weight in gathered], axis=1)
     pieces = jnp.split(projected, 8, axis=1)
     conv_mixed = conv_branch(pieces[0], pieces[1], pieces[2], convolution_taps)

time: 577 us -> 537 us (0.931)
  waiting for transfers between devices: 230 us -> 186 us
    all_gather x1, waiting for transfers between devices: 148 us -> 89.7 us  [side_by_side(): out = lax.all_gather(both, axis, axis=dim, tiled=True)]
    all_to_all x0 -> x1, waiting for transfers between devices: none -> 46.9 us  [on_device(): lax.all_to_all(jnp.stack([normed] * lax.axis_size('tp')), 'tp', 0, 0)]
    all_gather x1 -> x0, waiting for transfers between devices: 32.2 us -> none  [on_device(): piece = lax.all_gather(normed, 'tp', axis=0, tiled=True)]
  transfers between devices with their start and end apart: 6 -> 6, of which waited for: 4 -> 4; matrix products, arithmetic and copies ran while one was open for 53% -> 56% of each run, Pallas kernels for 0% -> 0%
where the time goes in v1:
time: 537 us; the launch traced here: 534 us
  other arithmetic  204 us (38%)
  waiting for transfers between devices  186 us (35%)
  matrix products  76.8 us (14%)
  local copies, waits for them, and re-layouts  36.6 us (7%)
  starting transfers between devices  16.2 us (3%)
  between operations  13.5 us (3%)
    another operation x32, other arithmetic, block_pass(): jax.scipy.linalg.solve_triangular(system, right_side, lower=True, unit_di...  157 us
    all_gather x1, waiting for transfers between devices, side_by_side(): out = lax.all_gather(both, axis, axis=dim, tiled=True)  89.7 us
    reduce_scatter x1, waiting for transfers between devices, on_device(): lax.psum_scatter((jnp.dot(conv_mixed, conv_whole, preferred_element_type=...  48.2 us
    all_to_all x1, waiting for transfers between devices, on_device(): lax.all_to_all(jnp.stack([normed] * lax.axis_size('tp')), 'tp', 0, 0)  46.9 us
    dot_general x7, matrix products, project(): jnp.dot(activations, weight, preferred_element_type=jnp.float32)  28.3 us
    mul x16, other arithmetic, block_pass(): ask_reads = queries * jnp.exp(cumulative - middle)  19.7 us
    another operation x16, other arithmetic, block_pass(): cumulative = jnp.cumsum(logarithm_decay, axis=0)  14.6 us
    dynamic_slice x32, local copies, waits for them, and re-layouts, on_device(): lax.scan(block_pass, initial_rows, tuple((in_blocks(array) for array in (...  12.7 us
  transfers between devices with their start and end apart: 6, of which 4 were waited for; matrix products, arithmetic and copies ran while one was open for 56% of the time, Pallas kernels for 0%

profile of v1, /device:TPU:8, one launch (start us, length us, event | category | flops | bytes accessed | tf_op | source)
XLA Modules:
  0.0 533.9 jit_solution(17773656821805206523)
XLA Ops:
  14.1 1.2 fusion.73
  15.3 2.5 stack.5
  17.9 4.7 all-to-all-start
  23.5 1.6 reshape_squeeze.3
  25.3 46.9 %all-to-all-done = bf16[8,128,2048]{2,1,0:T(8,128)(2,1)} async-done(((bf16[8,128,2048]{2,1,0:T(8,128)(2,1)}), bf16[8,128,2048]{2,1,0:T(8,128)(2,1)}, u32[]{:S(2)}, u32[]{:S(2)}) %all-to-all-start) | async-done | bytes 4194336 | tf_op jit(solution)/shard_map/all_to_all | solution.py:193
  72.2 89.7 %all-gather.3.cloned.1.call-done = bf16[2048,1024]{1,0:T(8,128)(2,1)} async-done(((bf16[32,1024]{1,0:T(8,128)(2,1)}), bf16[2048,1024]{1,0:T(8,128)(2,1)}) %all-gather.3.cloned.1.call-update) | async-done | bytes 4194320 | tf_op jit(solution)/shard_map/all_gather | solution.py:21
  161.9 3.8 bitcast_reduce_fusion
  167.8 4.3 fusion.51
  172.1 1.6 reshape.158
  173.8 4.4 fusion.55
  178.1 2.6 tanh.8
  180.8 4.3 fusion.50
  185.1 2.6 reshape.159
  187.7 4.3 fusion.53
  192.0 2.0 reshape.156
  194.0 2.7 negate_add_fusion
  196.7 4.0 divide_multiply_fusion
  200.8 237.3 %while.12 = (s32[]{:T(128)}, f32[2,128,64]{1,2,0:T(8,128)S(1)}, f32[16,64,2,128]{3,1,0,2:T(8,128)S(1)}, f32[16,64,2,64]{3,2,1,0:T(2,128)}, bf16[16,64,2,64]{3,2,...) while((s32[]{:T(128)}, f32[2,128,64]{1,2,0:T(8,128)S(1)}, ...), condition=%wide.region_4.5_spmd, body=%wide.region_2.4_spmd.sunk | while | flops 32329792 | bytes 2025073 | solution.py:228
  201.7 1.2 bitcast_multiply_fusion.9
  204.4 9.8 %custom-call.8 = f32[2,1,64,64]{2,3,1,0:T(8,128)S(1)} custom-call(f32[2,1,64,64]{3,2,1,0:T(8,128)S(1)} %fusion.193), custom_call_target="InvertDiagBlocksLowerTriangular" | custom-call | tf_op jit(solution)/shard_map/while/body/eval_jaxpr/jit(_solve_triangular)/vmap()/triangular_solve | solution.py:132
  216.5 1.2 bitcast_multiply_fusion.9
  219.2 9.8 %custom-call.8 = f32[2,1,64,64]{2,3,1,0:T(8,128)S(1)} custom-call(f32[2,1,64,64]{3,2,1,0:T(8,128)S(1)} %fusion.193), custom_call_target="InvertDiagBlocksLowerTriangular" | custom-call | tf_op jit(solution)/shard_map/while/body/eval_jaxpr/jit(_solve_triangular)/vmap()/triangular_solve | solution.py:132
  231.3 1.2 bitcast_multiply_fusion.9
  234.0 9.8 %custom-call.8 = f32[2,1,64,64]{2,3,1,0:T(8,128)S(1)} custom-call(f32[2,1,64,64]{3,2,1,0:T(8,128)S(1)} %fusion.193), custom_call_target="InvertDiagBlocksLowerTriangular" | custom-call | tf_op jit(solution)/shard_map/while/body/eval_jaxpr/jit(_solve_triangular)/vmap()/triangular_solve | solution.py:132
  246.2 1.3 bitcast_multiply_fusion.9
  248.9 9.9 %custom-call.8 = f32[2,1,64,64]{2,3,1,0:T(8,128)S(1)} custom-call(f32[2,1,64,64]{3,2,1,0:T(8,128)S(1)} %fusion.193), custom_call_target="InvertDiagBlocksLowerTriangular" | custom-call | tf_op jit(solution)/shard_map/while/body/eval_jaxpr/jit(_solve_triangular)/vmap()/triangular_solve | solution.py:132
  263.7 9.9 %custom-call.8 = f32[2,1,64,64]{2,3,1,0:T(8,128)S(1)} custom-call(f32[2,1,64,64]{3,2,1,0:T(8,128)S(1)} %fusion.193), custom_call_target="InvertDiagBlocksLowerTriangular" | custom-call | tf_op jit(solution)/shard_map/while/body/eval_jaxpr/jit(_solve_triangular)/vmap()/triangular_solve | solution.py:132
  275.8 1.2 bitcast_multiply_fusion.9
  278.5 9.8 %custom-call.8 = f32[2,1,64,64]{2,3,1,0:T(8,128)S(1)} custom-call(f32[2,1,64,64]{3,2,1,0:T(8,128)S(1)} %fusion.193), custom_call_target="InvertDiagBlocksLowerTriangular" | custom-call | tf_op jit(solution)/shard_map/while/body/eval_jaxpr/jit(_solve_triangular)/vmap()/triangular_solve | solution.py:132
  293.4 9.8 %custom-call.8 = f32[2,1,64,64]{2,3,1,0:T(8,128)S(1)} custom-call(f32[2,1,64,64]{3,2,1,0:T(8,128)S(1)} %fusion.193), custom_call_target="InvertDiagBlocksLowerTriangular" | custom-call | tf_op jit(solution)/shard_map/while/body/eval_jaxpr/jit(_solve_triangular)/vmap()/triangular_solve | solution.py:132
  308.2 9.8 %custom-call.8 = f32[2,1,64,64]{2,3,1,0:T(8,128)S(1)} custom-call(f32[2,1,64,64]{3,2,1,0:T(8,128)S(1)} %fusion.193), custom_call_target="InvertDiagBlocksLowerTriangular" | custom-call | tf_op jit(solution)/shard_map/while/body/eval_jaxpr/jit(_solve_triangular)/vmap()/triangular_solve | solution.py:132
  323.0 9.8 %custom-call.8 = f32[2,1,64,64]{2,3,1,0:T(8,128)S(1)} custom-call(f32[2,1,64,64]{3,2,1,0:T(8,128)S(1)} %fusion.193), custom_call_target="InvertDiagBlocksLowerTriangular" | custom-call | tf_op jit(solution)/shard_map/while/body/eval_jaxpr/jit(_solve_triangular)/vmap()/triangular_solve | solution.py:132
  337.9 9.8 %custom-call.8 = f32[2,1,64,64]{2,3,1,0:T(8,128)S(1)} custom-call(f32[2,1,64,64]{3,2,1,0:T(8,128)S(1)} %fusion.193), custom_call_target="InvertDiagBlocksLowerTriangular" | custom-call | tf_op jit(solution)/shard_map/while/body/eval_jaxpr/jit(_solve_triangular)/vmap()/triangular_solve | solution.py:132
  352.7 9.8 %custom-call.8 = f32[2,1,64,64]{2,3,1,0:T(8,128)S(1)} custom-call(f32[2,1,64,64]{3,2,1,0:T(8,128)S(1)} %fusion.193), custom_call_target="InvertDiagBlocksLowerTriangular" | custom-call | tf_op jit(solution)/shard_map/while/body/eval_jaxpr/jit(_solve_triangular)/vmap()/triangular_solve | solution.py:132
  364.8 1.2 bitcast_multiply_fusion.9
  367.5 9.8 %custom-call.8 = f32[2,1,64,64]{2,3,1,0:T(8,128)S(1)} custom-call(f32[2,1,64,64]{3,2,1,0:T(8,128)S(1)} %fusion.193), custom_call_target="InvertDiagBlocksLowerTriangular" | custom-call | tf_op jit(solution)/shard_map/while/body/eval_jaxpr/jit(_solve_triangular)/vmap()/triangular_solve | solution.py:132
  382.3 9.8 %custom-call.8 = f32[2,1,64,64]{2,3,1,0:T(8,128)S(1)} custom-call(f32[2,1,64,64]{3,2,1,0:T(8,128)S(1)} %fusion.193), custom_call_target="InvertDiagBlocksLowerTriangular" | custom-call | tf_op jit(solution)/shard_map/while/body/eval_jaxpr/jit(_solve_triangular)/vmap()/triangular_solve | solution.py:132
  397.2 9.8 %custom-call.8 = f32[2,1,64,64]{2,3,1,0:T(8,128)S(1)} custom-call(f32[2,1,64,64]{3,2,1,0:T(8,128)S(1)} %fusion.193), custom_call_target="InvertDiagBlocksLowerTriangular" | custom-call | tf_op jit(solution)/shard_map/while/body/eval_jaxpr/jit(_solve_triangular)/vmap()/triangular_solve | solution.py:132
  409.3 1.2 bitcast_multiply_fusion.9
  412.0 9.8 %custom-call.8 = f32[2,1,64,64]{2,3,1,0:T(8,128)S(1)} custom-call(f32[2,1,64,64]{3,2,1,0:T(8,128)S(1)} %fusion.193), custom_call_target="InvertDiagBlocksLowerTriangular" | custom-call | tf_op jit(solution)/shard_map/while/body/eval_jaxpr/jit(_solve_triangular)/vmap()/triangular_solve | solution.py:132
  426.8 9.8 %custom-call.8 = f32[2,1,64,64]{2,3,1,0:T(8,128)S(1)} custom-call(f32[2,1,64,64]{3,2,1,0:T(8,128)S(1)} %fusion.193), custom_call_target="InvertDiagBlocksLowerTriangular" | custom-call | tf_op jit(solution)/shard_map/while/body/eval_jaxpr/jit(_solve_triangular)/vmap()/triangular_solve | solution.py:132
  439.3 7.5 %all-to-all-start.1 = ((bf16[16,256,64]{1,2,0:T(8,128)(2,1)}), bf16[16,256,64]{1,2,0:T(8,128)(2,1)S(1)}, u32[]{:S(2)}, u32[]{:S(2)}) async-start(bf16[16,256,64]{1,2,0:T(8,128)(2,1)} %broadcast_in_dim.79), calls=%async_computation.1 | async-start | bytes 1048576 | tf_op jit(solution)/shard_map/all_to_all | solution.py:27
  446.9 3.5 fusion.58
  450.4 3.6 fusion.57
  454.0 3.8 collective-permute-start
  459.1 10.1 %fusion.80 = f32[1024,2048]{1,0:T(8,128)} fusion(bf16[2048,256]{1,0:T(8,128)(2,1)} %all-gather.5.cloned.1.call-done, f32[2,128]{1,0:T(2,128)S(1)} %collective-permute-done, f32[1024,128]{1,0:T(8,128)S(1)} %fusion.57, bf16[1024,2048]{1,0:T(8,128)(2,1)} %bitcast.15, bf16[2048,1024]{1,0:T(8,128)(2,1)} %all-gather.3.cloned.1.call-done, ...), kind=kOutput, calls=%fused_computation.126 | convolution fusion | flops 1075183616 | bytes 14158336 | tf_op jit(solution)/shard_map/dot_general | solution.py:262
  472.3 6.8 %add_convert_fusion = bf16[1024,2048]{1,0:T(8,128)(2,1)} fusion(f32[1024,2048]{1,0:T(8,128)} %fusion.80, bf16[1024,128]{0,1:T(8,128)(2,1)S(1)} %bitcast.178, bf16[2048,256]{1,0:T(8,128)(2,1)} %all-gather.5.cloned.1.call-done), kind=kOutput, calls=%fused_computation.74 | convolution fusion | flops 541065216 | bytes 13369344 | tf_op jit(solution)/shard_map/dot_general | solution.py:263
  479.1 48.2 %reduce-scatter.2.cloned.1.call-done = bf16[128,2048]{1,0:T(8,128)(2,1)} async-done(((bf16[1024,2048]{1,0:T(8,128)(2,1)}), bf16[128,2048]{1,0:T(8,128)(2,1)}) %reduce-scatter.2.cloned.1.call-update) | async-done | bytes 524304 | tf_op jit(solution)/shard_map/reduce_scatter | solution.py:260
  (378 shorter events, 86.1 us)
Async XLA Ops:
  6.5 465.1 %copy-start = (f32[1,2,64,64]{3,2,1,0:T(8,128)S(1)}, f32[1,2,64,64]{3,2,1,0:T(8,128)}, u32[]{:S(2)}) copy-start(f32[1,2,64,64]{3,2,1,0:T(8,128)} %param.34) | copy-start | bytes 98308
  6.5 155.4 %all-gather.3.cloned.1.call-start = ((), (), s32[]{:S(2)}) async-start(), calls=%async_computation.3 | async-start | bytes 4259840 | tf_op jit(solution)/shard_map/all_gather | solution.py:21
  12.2 0.6 copy-start.2
  17.8 4.8 copy-start.3
  17.8 4.8 copy-start.4
  17.8 5.5 %copy-start.6 = (f32[128]{0:T(128)S(1)}, f32[128]{0:T(128)}, u32[]{:S(2)}) copy-start(f32[128]{0:T(128)} %param.32) | copy-start | bytes 1540
  17.8 5.6 %copy-start.1 = (f32[1,1024,128]{2,1,0:T(8,128)S(1)}, f32[1,1024,128]{2,1,0:T(8,128)}, u32[]{:S(2)}) copy-start(f32[1,1024,128]{2,1,0:T(8,128)} %param.33) | copy-start | bytes 1572868
  17.8 7.2 %copy-start.7 = (f32[128]{0:T(128)S(1)}, f32[128]{0:T(128)}, u32[]{:S(2)}) copy-start(f32[128]{0:T(128)} %param.31) | copy-start | bytes 1540
  17.9 54.4 %all-to-all-start = ((bf16[8,128,2048]{2,1,0:T(8,128)(2,1)}), bf16[8,128,2048]{2,1,0:T(8,128)(2,1)}, u32[]{:S(2)}, u32[]{:S(2)}) async-start(bf16[8,128,2048]{2,1,0:T(8,128)(2,1)} %stack.5), calls=%async_computation | async-start | bytes 8388608 | tf_op jit(solution)/shard_map/all_to_all | solution.py:193
  22.6 435.7 %all-gather.5.cloned.1.call-start = ((), (), s32[]{:S(2)}) async-start(), calls=%async_computation.4 | async-start | bytes 1064960 | tf_op jit(solution)/shard_map/all_gather | solution.py:76
  200.7 246.1 %copy-start.5 = (f32[3,128]{1,0:T(4,128)S(1)}, f32[3,128]{1,0:T(4,128)}, u32[]{:S(2)}) copy-start(f32[3,128]{1,0:T(4,128)} %param.25) | copy-start | bytes 4612
  439.3 29.9 %all-to-all-start.1 = ((bf16[16,256,64]{1,2,0:T(8,128)(2,1)}), bf16[16,256,64]{1,2,0:T(8,128)(2,1)S(1)}, u32[]{:S(2)}, u32[]{:S(2)}) async-start(bf16[16,256,64]{1,2,0:T(8,128)(2,1)} %broadcast_in_dim.79), calls=%async_computation.1 | async-start | bytes 1048576 | tf_op jit(solution)/shard_map/all_to_all | solution.py:27
  446.8 80.5 %reduce-scatter.2.cloned.1.call-start = ((), (), s32[]{:S(2)}) async-start(), calls=%async_computation.5 | async-start | bytes 4718592 | tf_op jit(solution)/shard_map/reduce_scatter | solution.py:260
  450.4 7.4 %copy-start.8 = (f32[128]{0:T(128)S(1)}, f32[128]{0:T(128)}, u32[]{:S(2)}) copy-start(f32[128]{0:T(128)} %param.35) | copy-start | bytes 1540
  454.0 5.1 collective-permute-start
Sparse Core Ops, SparseCore 0:
  13.0 148.9 all-gather.2
  164.9 137.2 all-gather.4
  479.2 48.0 reduce-scatter.1
